TPU v7x, 32 devices: a whole 2x2x4 slice. The times are simulated.
32 devices in a mesh: grp: 2 (over y), sp: 4 (over z), tp: 4 (over x, core).
Axes of the slice: x: 2, y: 2, z: 4, core: 2. Of those that a mesh axis runs over, the one named last changes fastest.
Arguments:
- ssm_input: bfloat16 [1024, 1024], P(('grp', 'sp'), 'tp'), parts along dimension 0, may hold values from -6 to 6
- residual_in: bfloat16 [1024, 2048], P(('grp', 'sp')), parts along dimension 0, may hold values from -4 to 4
- log_step: float32 [64], P('tp'), may hold values from -6.91 to -2.3
- decay_real: float32 [64, 64], P('tp'), may hold values from -34 to 0, as said below
- freq: float32 [64, 64], P('tp'), may hold values from 0.5 to 8
- in_real: float32 [64, 64, 16], P('tp'), may hold values from -1 to 1
- in_imag: float32 [64, 64, 16], P('tp'), may hold values from -1 to 1
- out_real: float32 [64, 16, 64], P('tp'), may hold values from -0.5 to 0.5
- out_imag: float32 [64, 16, 64], P('tp'), may hold values from -0.5 to 0.5
- skip: float32 [1024], P('tp'), may hold values from -3 to 3
- w_glu: bfloat16 [1024, 1024], replicated, may hold values from -0.1875 to 0.1875
- b_glu: float32 [1024], replicated, may hold values from -3 to 3
- w_branch: bfloat16 [1024, 2048], replicated, may hold values from -0.1875 to 0.1875
- norm_gain: float32 [2048], replicated, may hold values from 0.1 to 1.9
- w_gate: bfloat16 [2048, 5632], P('sp', 'tp'), may hold values from -0.125 to 0.125
- w_up: bfloat16 [2048, 5632], P('sp', 'tp'), may hold values from -0.125 to 0.125
- w_down: bfloat16 [5632, 2048], P('tp', 'sp'), may hold values from -0.078125 to 0.078125
Outputs:
- mixed: bfloat16 [1024, 2048], P(('grp', 'sp', 'tp')), parts along dimension 0
There are 2 independent parts, one for each index of `grp`. A program takes and returns all parts, laid end to end along the dimension named above; an argument that names none is the same for every part. Nothing has to cross between parts.
Inputs may be any that keep to these rules, and one draw needn't show every extreme that they name: `decay_real`: negative in every entry.
All inputs are finite; a program needn't handle non-finite values.
Results may differ from a plain program's by a relative error of at most 0.015.
Values may be sent and summed in bfloat16 or wider, within the bound.
A program may use at most 128 MiB of HBM per device.

v0:
```python
import math

import jax
import jax.numpy as jnp
from jax import lax
from jax.sharding import PartitionSpec as P

EPS = 1e-06


def prefix(shard, axis, combine, identity):
    count, place = (lax.axis_size(axis), lax.axis_index(axis))
    everything = jax.tree.map(lambda part: lax.all_gather(part, axis), shard)
    start = jax.tree.map(
        lambda part, zero: jnp.broadcast_to(jnp.asarray(zero, part.dtype), part.shape),
        shard,
        identity,
    )

    def lap(k, before):
        reached = k < place
        new = combine(before, jax.tree.map(lambda part: part[k], everything))
        return jax.tree.map(lambda a, b: jnp.where(reached, a, b), new, before)

    return lax.fori_loop(0, count, lap, start)


def discretize(log_step, decay_real, freq, in_real, in_imag):
    step_size = jnp.exp(log_step)[:, None]
    magnitude = jnp.exp(decay_real * step_size)
    abar_re = magnitude * jnp.cos(freq * step_size)
    abar_im = magnitude * jnp.sin(freq * step_size)
    denominator = decay_real * decay_real + freq * freq
    less_re = abar_re - 1.0
    hold_re = ((less_re * decay_real + abar_im * freq) / denominator)[..., None]
    hold_im = ((abar_im * decay_real - less_re * freq) / denominator)[..., None]
    bbar_re = hold_re * in_real - hold_im * in_imag
    bbar_im = hold_re * in_imag + hold_im * in_real
    return (step_size, abar_re, abar_im, bbar_re, bbar_im)


def powers(decay_real, freq, step_size, length):
    steps_up = (jnp.arange(length, dtype=jnp.int32) + 1).astype(jnp.float32)[:, None, None]
    magnitude = jnp.exp((decay_real * step_size)[None] * steps_up)
    phase = (freq * step_size)[None] * steps_up
    return (magnitude * jnp.cos(phase), magnitude * jnp.sin(phase))


def compose(earlier, later):
    a1r, a1i, b1r, b1i = earlier
    a2r, a2i, b2r, b2i = later
    return (
        a2r * a1r - a2i * a1i,
        a2r * a1i + a2i * a1r,
        a2r * b1r - a2i * b1i + b2r,
        a2r * b1i + a2i * b1r + b2i,
    )


def local_states(inputs, decay_real, freq, step_size, bbar_re, bbar_im):
    highest = lax.Precision.HIGHEST
    tok_rows, group_count, unused = inputs.shape
    lanes = group_count * decay_real.shape[1]
    drive_re = jnp.einsum("lgm,gpm->lgp", inputs, bbar_re, precision=highest).reshape(
        tok_rows, lanes
    )
    drive_im = jnp.einsum("lgm,gpm->lgp", inputs, bbar_im, precision=highest).reshape(
        tok_rows, lanes
    )
    span = math.gcd(tok_rows, 16)
    spans = tok_rows // span
    rate = (decay_real * step_size).reshape(lanes)
    turn = (freq * step_size).reshape(lanes)
    later = jnp.arange(span, dtype=jnp.int32)[:, None]
    earlier = jnp.arange(span, dtype=jnp.int32)[None, :]
    lag = (later - earlier).astype(jnp.float32)
    causal = (later >= earlier)[..., None]
    lag_pos = jnp.maximum(lag, 0.0)[..., None]
    table_mag = jnp.exp(rate[None, None] * lag_pos)
    table_re = jnp.where(causal, table_mag * jnp.cos(turn[None, None] * lag_pos), 0.0)
    table_im = jnp.where(causal, table_mag * jnp.sin(turn[None, None] * lag_pos), 0.0)
    block_re = drive_re.reshape(spans, 1, span, lanes)
    block_im = drive_im.reshape(spans, 1, span, lanes)
    inner_re = jnp.sum(table_re[None] * block_re - table_im[None] * block_im, axis=2)
    inner_im = jnp.sum(table_re[None] * block_im + table_im[None] * block_re, axis=2)
    steps_up = (jnp.arange(span, dtype=jnp.int32) + 1).astype(jnp.float32)[:, None]
    pow_mag = jnp.exp(rate[None] * steps_up)
    pow_re = pow_mag * jnp.cos(turn[None] * steps_up)
    pow_im = pow_mag * jnp.sin(turn[None] * steps_up)
    span_re = pow_re[-1]
    span_im = pow_im[-1]

    def carry_step(entering, ends):
        next_re = span_re * entering[0] - span_im * entering[1] + ends[0]
        next_im = span_re * entering[1] + span_im * entering[0] + ends[1]
        return ((next_re, next_im), entering)

    zeros = jnp.zeros((lanes,), jnp.float32)
    unused_carry, entering = lax.scan(
        carry_step, (zeros, zeros), (inner_re[:, -1], inner_im[:, -1])
    )
    state_re = inner_re + pow_re[None] * entering[0][:, None] - pow_im[None] * entering[1][:, None]
    state_im = inner_im + pow_re[None] * entering[1][:, None] + pow_im[None] * entering[0][:, None]
    shape = (tok_rows, group_count, decay_real.shape[1])
    return (state_re.reshape(shape), state_im.reshape(shape))


def readout(state_re, state_im, out_real, out_imag, skip_mat, inputs):
    highest = lax.Precision.HIGHEST
    values = (
        jnp.einsum("lgp,gmp->lgm", state_re, out_real, precision=highest)
        - jnp.einsum("lgp,gmp->lgm", state_im, out_imag, precision=highest)
        + skip_mat[None] * inputs
    )
    values = jax.nn.gelu(values)
    return values.reshape(values.shape[0], -1).astype(jnp.bfloat16)


def row_norm(stream, norm_gain):
    scale_rows = lax.rsqrt(jnp.mean(stream * stream, axis=-1, keepdims=True) + EPS)
    return (stream * scale_rows * norm_gain).astype(jnp.bfloat16)


def per_device(
    ssm_input,
    residual_in,
    log_step,
    decay_real,
    freq,
    in_real,
    in_imag,
    out_real,
    out_imag,
    skip,
    w_glu,
    b_glu,
    w_branch,
    norm_gain,
    w_gate,
    w_up,
    w_down,
):
    tok_rows, width_local = ssm_input.shape
    group_count = log_step.shape[0]
    group_size = in_real.shape[2]
    tp_count = lax.axis_size("tp")
    tp_index = lax.axis_index("tp")
    own_rows = tok_rows // tp_count
    step_size, abar_re, abar_im, bbar_re, bbar_im = discretize(
        log_step, decay_real, freq, in_real, in_imag
    )
    pow_re, pow_im = powers(decay_real, freq, step_size, tok_rows)
    inputs = ssm_input.astype(jnp.float32).reshape(tok_rows, group_count, group_size)
    local_re, local_im = local_states(inputs, decay_real, freq, step_size, bbar_re, bbar_im)
    identity = (
        jnp.ones_like(abar_re),
        jnp.zeros_like(abar_re),
        jnp.zeros_like(abar_re),
        jnp.zeros_like(abar_re),
    )
    carried = prefix((pow_re[-1], pow_im[-1], local_re[-1], local_im[-1]), "sp", compose, identity)
    state_re = local_re + pow_re * carried[2][None] - pow_im * carried[3][None]
    state_im = local_im + pow_re * carried[3][None] + pow_im * carried[2][None]
    mixer_out = readout(
        state_re, state_im, out_real, out_imag, skip.reshape(group_count, group_size), inputs
    )
    mixer_rows = lax.all_to_all(mixer_out, "tp", split_axis=0, concat_axis=1, tiled=True)
    glu_pre = jnp.dot(mixer_rows, w_glu, preferred_element_type=jnp.float32) + b_glu
    gated = (mixer_rows.astype(jnp.float32) * jax.nn.sigmoid(glu_pre)).astype(jnp.bfloat16)
    residual_own = lax.dynamic_slice_in_dim(residual_in, tp_index * own_rows, own_rows, 0)
    stream = residual_own.astype(jnp.float32) + jnp.dot(
        gated, w_branch, preferred_element_type=jnp.float32
    )
    normed = row_norm(stream, norm_gain)
    normed_all = lax.all_gather(normed, "tp", axis=0, tiled=True)
    gate_sum = jnp.dot(
        normed_all,
        lax.all_gather(w_gate, "sp", axis=0, tiled=True),
        preferred_element_type=jnp.float32,
    )
    up_sum = jnp.dot(
        normed_all,
        lax.all_gather(w_up, "sp", axis=0, tiled=True),
        preferred_element_type=jnp.float32,
    )
    hidden = (jax.nn.silu(gate_sum) * up_sum).astype(jnp.bfloat16)
    down_whole = lax.all_gather(w_down, "sp", axis=1, tiled=True)
    summed = lax.psum_scatter(
        jnp.dot(hidden, down_whole, preferred_element_type=jnp.float32).astype(jnp.bfloat16),
        "tp",
        scatter_dimension=0,
        tiled=True,
    ).astype(jnp.float32)
    return (stream + summed).astype(jnp.bfloat16)


def solution(mesh):
    placed = (
        P(("grp", "sp"), "tp"),
        P(("grp", "sp"), None),
        P("tp"),
        P("tp", None),
        P("tp", None),
        P("tp", None, None),
        P("tp", None, None),
        P("tp", None, None),
        P("tp", None, None),
        P("tp"),
        P(),
        P(),
        P(),
        P(),
        P("sp", "tp"),
        P("sp", "tp"),
        P("tp", "sp"),
    )
    return jax.shard_map(
        per_device,
        mesh=mesh,
        in_specs=placed,
        out_specs=P(("grp", "sp", "tp"), None),
        check_vma=False,
    )
```

profile of v0, /device:TPU:0, one launch (start us, length us, event | category | flops | bytes accessed | tf_op | source)
XLA Modules:
  0.0 368.5 jit_solution(1587325660411894880)
XLA Ops:
  11.2 2.4 convolution_bitcast_fusion.1
  13.6 2.4 convolution_bitcast_fusion
  21.6 4.0 %fusion.14 = (f32[16,16,1024]{2,1,0:T(8,128)S(1)}, f32[16,16,1024]{2,1,0:T(8,128)S(1)}) fusion(f32[1024]{0:T(1024)S(1)} %mul.483, f32[16,16]{1,0:T(8,128)S(1)} %convert_maximum_fusion, f32[1024]{0:T(1024)S(1)} %mul.478, pred[16,16]{1,0:T(8,128)(4,1)S(1)} %iota_compare_fusion), kind=kLoop, calls=%fused_computation.39 | loop fusion | flops 1572864 | bytes 2106624 | tf_op jit(solution)/shard_map/jit(_where)/select_n | solution.py:80
  25.6 6.2 %add_reduce_fusion = (f32[8,16,1024]{2,1,0:T(8,128)S(1)}, f32[8,16,1024]{2,1,0:T(8,128)S(1)}) fusion(f32[8,16,1024]{2,1,0:T(8,128)} %mul.507, f32[16,16,1024]{2,1,0:T(8,128)S(1)} %get-tuple-element.302, f32[8,16,1024]{2,1,0:T(8,128)} %mul.500, f32[16,16,1024]{2,1,0:T(8,128)S(1)} %get-tuple-element.301), kind=kLoop, calls=%fused_computation.16 | loop fusion | flops 16515072 | bytes 4194304 | tf_op jit(solution)/shard_map/reduce_sum | solution.py:85
  32.2 22.7 %while.33 = (s32[]{:T(128)}, f32[1024]{0:T(1024)S(1)}, f32[1024]{0:T(1024)S(1)}, f32[8,1024]{1,0:T(8,128)}, f32[8,1024]{1,0:T(8,128)}, /*index=5*/f32[1024]{0:T(...) while((s32[]{:T(128)}, f32[1024]{0:T(1024)S(1)}, ...), condition=%wide.region_3.4_spmd.clone, body=%wide.region_2.3_spmd.clone.sunk | while | flops 10243 | bytes 90243 | solution.py:99
  54.9 1.9 multiply_add_fusion.1
  58.2 2.3 add.177
  61.2 3.9 %fusion.18 = (f32[128,16,64]{2,1,0:T(8,128)S(1)}, f32[128,16,64]{2,1,0:T(8,128)S(1)}) fusion(f32[16,64]{1,0:T(8,128)S(1)} %get-tuple-element.310, f32[128]{0:T(128)S(1)} %add_convert_fusion.1, f32[16,64]{1,0:T(8,128)S(1)} %get-tuple-element.309), kind=kLoop, calls=%fused_computation.43 | loop fusion | flops 524288 | bytes 1057280 | tf_op jit(solution)/shard_map/mul | solution.py:46
  65.2 16.7 %all_gather.26 = f32[4,16,64]{2,1,0:T(8,128)S(1)} all-gather(f32[1,16,64]{2,1,0:T(8,128)S(1)} %slice.38), channel_id=1, replica_groups=mesh['grp'=2,'sp'=4,'tp'=4] {'sp'}, dimensions={0}, use_global_device_ids=true | all-gather | bytes 20480 | tf_op jit(solution)/shard_map/all_gather | solution.py:13
  81.9 17.5 %all_gather.27 = f32[4,16,64]{2,1,0:T(8,128)S(1)} all-gather(f32[1,16,64]{2,1,0:T(8,128)S(1)} %slice.39), channel_id=1, replica_groups=mesh['grp'=2,'sp'=4,'tp'=4] {'sp'}, dimensions={0}, use_global_device_ids=true | all-gather | bytes 20480 | tf_op jit(solution)/shard_map/all_gather | solution.py:13
  99.5 15.9 %all_gather.24 = f32[4,16,64]{2,1,0:T(8,128)S(1)} all-gather(f32[1,16,64]{2,1,0:T(8,128)S(1)} %slice.36), channel_id=1, replica_groups=mesh['grp'=2,'sp'=4,'tp'=4] {'sp'}, dimensions={0}, use_global_device_ids=true | all-gather | bytes 20480 | tf_op jit(solution)/shard_map/all_gather | solution.py:13
  115.4 13.9 %all_gather.25 = f32[4,16,64]{2,1,0:T(8,128)S(1)} all-gather(f32[1,16,64]{2,1,0:T(8,128)S(1)} %slice.37), channel_id=1, replica_groups=mesh['grp'=2,'sp'=4,'tp'=4] {'sp'}, dimensions={0}, use_global_device_ids=true | all-gather | bytes 20480 | tf_op jit(solution)/shard_map/all_gather | solution.py:13
  129.4 5.4 %multiply_add_fusion = (f32[128,16,64]{2,1,0:T(8,128)S(1)}, f32[128,16,64]{2,1,0:T(8,128)S(1)}) fusion(f32[128,16,64]{2,1,0:T(8,128)} %add.177, f32[16,64]{1,0:T(8,128)S(1)} %get-tuple-element.196, f32[16,64]{1,0:T(8,128)S(1)} %get-tuple-element.195, f32[16,64]{1,0:T(8,128)S(1)} %get-tuple-element.310, f32[128]{0:T(128)S(1)} %add_convert_fusion.1, ...), kind=kLoop, calls=%fused_computation.47 | loop fusion | flops 1572864 | bytes 2114048 | tf_op jit(solution)/shard_map/add | solution.py:163
  134.9 1.9 fusion.20
  136.8 2.9 fusion.32
  140.7 3.3 all-to-all-start
  144.0 4.0 %all-to-all-done = bf16[4,32,256]{2,1,0:T(8,128)(2,1)S(1)} async-done(((bf16[4,32,256]{2,1,0:T(8,128)(2,1)}), bf16[4,32,256]{2,1,0:T(8,128)(2,1)S(1)}, u32[]{:S(2)}, u32[]{:S(2)}) %all-to-all-start) | async-done | bytes 65568 | tf_op jit(solution)/shard_map/all_to_all | solution.py:167
  148.1 3.5 multiply_reduce_fusion
  151.7 7.0 %all_gather.28 = bf16[128,2048]{1,0:T(8,128)(2,1)S(1)} all-gather(bf16[32,2048]{1,0:T(8,128)(2,1)S(1)} %multiply_convert_fusion), channel_id=1, replica_groups=mesh['grp'=2,'sp'=4,'tp'=4] {'tp'}, dimensions={0}, use_global_device_ids=true | all-gather | bytes 655360 | tf_op jit(solution)/shard_map/all_gather | solution.py:175
  158.7 4.6 %fusion.53 = f32[128,1408]{1,0:T(8,128)} fusion(bf16[128,2048]{1,0:T(8,128)(2,1)S(1)} %all_gather.28, bf16[2048,1408]{1,0:T(8,128)(2,1)} %all-gather.4.cloned.1.call-done), kind=kOutput, calls=%fused_computation.100 | convolution fusion | flops 738197504 | bytes 7012352 | tf_op jit(solution)/shard_map/dot_general | solution.py:176
  163.3 63.2 %all-gather.6.cloned.1.call-done = bf16[2048,1408]{1,0:T(8,128)(2,1)} async-done(((bf16[512,1408]{1,0:T(8,128)(2,1)}), bf16[2048,1408]{1,0:T(8,128)(2,1)}) %all-gather.6.cloned.1.call-update) | async-done | bytes 5767184 | tf_op jit(solution)/shard_map/all_gather | solution.py:183
  226.5 106.5 %all-gather.8.cloned.1.call-done = bf16[1408,2048]{1,0:T(8,128)(2,1)} async-done(((bf16[1408,512]{1,0:T(8,128)(2,1)}), bf16[1408,2048]{1,0:T(8,128)(2,1)}) %all-gather.8.cloned.1.call-update) | async-done | bytes 5767184 | tf_op jit(solution)/shard_map/all_gather | solution.py:187
  333.1 7.2 %convolution_convert_fusion = bf16[128,2048]{1,0:T(8,128)(2,1)} fusion(bf16[1408,2048]{1,0:T(8,128)(2,1)} %all-gather.8.cloned.1.call-done, bf16[128,2048]{1,0:T(8,128)(2,1)S(1)} %all_gather.28, bf16[2048,1408]{1,0:T(8,128)(2,1)} %all-gather.6.cloned.1.call-done, f32[128,1408]{1,0:T(8,128)} %fusion.53), kind=kOutput, calls=%fused_computation.20 | convolution fusion | flops 1477738496 | bytes 13303808 | tf_op jit(solution)/shard_map/dot_general | solution.py:189
  340.3 20.0 %reduce-scatter.2.cloned.1.call-done = bf16[32,2048]{1,0:T(8,128)(2,1)} async-done(((bf16[128,2048]{1,0:T(8,128)(2,1)}), bf16[32,2048]{1,0:T(8,128)(2,1)}) %reduce-scatter.2.cloned.1.call-update) | async-done | bytes 131088 | tf_op jit(solution)/shard_map/reduce_scatter | solution.py:188
  (101 shorter events, 38.2 us)
Async XLA Ops:
  6.5 141.5 %copy-start = (bf16[1024,1024]{1,0:T(8,128)(2,1)S(1)}, bf16[1024,1024]{1,0:T(8,128)(2,1)}, u32[]{:S(2)}) copy-start(bf16[1024,1024]{1,0:T(8,128)(2,1)} %param.31) | copy-start | bytes 6291460
  6.5 152.2 %all-gather.4.cloned.1.call-start = ((), (), s32[]{:S(2)}) async-start(), calls=%async_computation.2 | async-start | bytes 7208960 | tf_op jit(solution)/shard_map/all_gather | solution.py:178
  7.3 219.3 %all-gather.6.cloned.1.call-start = ((), (), s32[]{:S(2)}) async-start(), calls=%async_computation.3 | async-start | bytes 7208960 | tf_op jit(solution)/shard_map/all_gather | solution.py:183
  8.0 325.1 %all-gather.8.cloned.1.call-start = ((), (), s32[]{:S(2)}) async-start(), calls=%async_computation.4 | async-start | bytes 7208960 | tf_op jit(solution)/shard_map/all_gather | solution.py:187
  25.5 39.6 %copy-start.4 = (f32[256]{0:T(256)S(1)}, f32[256]{0:T(256)}, u32[]{:S(2)}) copy-start(f32[256]{0:T(256)} %param.30) | copy-start | bytes 3076
  54.9 80.0 %copy-start.1 = (f32[16,16,64]{2,1,0:T(8,128)S(1)}, f32[16,16,64]{2,1,0:T(8,128)}, u32[]{:S(2)}) copy-start(f32[16,16,64]{2,1,0:T(8,128)} %param.28) | copy-start | bytes 196612
  60.5 87.6 %copy-start.3 = (f32[1024]{0:T(1024)S(1)}, f32[1024]{0:T(1024)}, u32[]{:S(2)}) copy-start(f32[1024]{0:T(1024)} %param.32) | copy-start | bytes 12292
  134.9 16.8 %copy-start.2 = (f32[2048]{0:T(1024)S(1)}, f32[2048]{0:T(1024)}, u32[]{:S(2)}) copy-start(f32[2048]{0:T(1024)} %param.34) | copy-start | bytes 24580
  140.7 7.4 %all-to-all-start = ((bf16[4,32,256]{2,1,0:T(8,128)(2,1)}), bf16[4,32,256]{2,1,0:T(8,128)(2,1)S(1)}, u32[]{:S(2)}, u32[]{:S(2)}) async-start(bf16[4,32,256]{2,1,0:T(8,128)(2,1)} %copy.47), calls=%async_computation | async-start | bytes 131072 | tf_op jit(solution)/shard_map/all_to_all | solution.py:167
  144.0 216.4 %reduce-scatter.2.cloned.1.call-start = ((), (), s32[]{:S(2)}) async-start(), calls=%async_computation.5 | async-start | bytes 655360 | tf_op jit(solution)/shard_map/reduce_scatter | solution.py:188
Sparse Core Ops, SparseCore 0:
  8.9 110.9 all-gather.3
  121.5 105.0 all-gather.5
  228.1 104.9 all-gather.7
  340.5 19.8 reduce-scatter.1
where the time goes:
time: 370 us; the launch traced here: 368 us
  waiting for transfers between devices  196 us (53%)
  blocking collectives  71 us (19%)
  local copies, waits for them, and re-layouts  35 us (9%)
  matrix products  24.9 us (7%)
  other arithmetic  24.5 us (7%)
  between operations  13.4 us (4%)
    all_gather x1, waiting for transfers between devices, per_device(): down_whole = lax.all_gather(w_down, 'sp', axis=1, tiled=True)  107 us
    all_gather x4, blocking collectives, prefix(): everything = jax.tree.map(lambda part: lax.all_gather(part, axis), shard)  64 us
    all_gather x1, waiting for transfers between devices, per_device(): lax.all_gather(w_up, 'sp', axis=0, tiled=True)  63.2 us
    dynamic_update_slice x16, local copies, waits for them, and re-layouts, local_states(): lax.scan(carry_step, (zeros, zeros), (inner_re[:, -1], inner_im[:, -1]))  22.3 us
    reduce_scatter x1, waiting for transfers between devices, per_device(): lax.psum_scatter(jnp.dot(hidden, down_whole, preferred_element_type=jnp.f...  20 us
  transfers between devices with their start and end apart: 5, of which 4 were waited for; matrix products, arithmetic and copies ran while one was open for 21% of the time, Pallas kernels for 0%

commit v1 on v0

--- a/solution.py
+++ b/solution.py
@@ -1,8 +1,11 @@
+import functools
 import math
 
 import jax
 import jax.numpy as jnp
 from jax import lax
+from jax.experimental import pallas as pl
+from jax.experimental.pallas import tpu as pltpu
 from jax.sharding import PartitionSpec as P
 
 EPS = 1e-06
@@ -121,7 +124,7 @@
     return (stream * scale_rows * norm_gain).astype(jnp.bfloat16)
 
 
-def per_device(
+def gathered_weights(
     ssm_input,
     residual_in,
     log_step,
@@ -194,6 +197,412 @@
     return (stream + summed).astype(jnp.bfloat16)
 
 
+MESH = pl.DeviceIdType.MESH
+F32 = jnp.float32
+BF16 = jnp.bfloat16
+NT = (((1,), (1,)), ((), ()))
+
+
+def greet(n_sp, n_tp, me_s, me_t):
+    barrier = pltpu.get_barrier_semaphore()
+    for d in range(1, n_sp):
+        pl.semaphore_signal(
+            barrier, inc=1, device_id={"sp": lax.rem(me_s + d, n_sp)}, device_id_type=MESH
+        )
+    for d in range(1, n_tp):
+        pl.semaphore_signal(
+            barrier, inc=1, device_id={"tp": lax.rem(me_t + d, n_tp)}, device_id_type=MESH
+        )
+    pl.semaphore_wait(barrier, n_sp + n_tp - 2)
+
+
+def mixer_kernel(
+    n_sp, n_tp,
+    u_ref, res_ref, ls_ref, dec_ref, frq_ref, inr_ref, ini_ref, outr_ref, outi_ref,
+    skip_ref, wglu_ref, bglu_ref, wbr_ref, gain_ref,
+    normed_ref, stream_ref,
+    wglu, wbr, res, coef, xr, xi, pr_all, pi_all, fin, fin_in, mo, rows_in, glu,
+    load_sem, fs, fr, rs, rr,
+):
+    me_s, me_t = lax.axis_index("sp"), lax.axis_index("tp")
+    tok, width = u_ref.shape
+    groups, states = dec_ref.shape
+    group = width // groups
+    lanes = groups * states
+    own = tok // n_tp
+    loads = [
+        pltpu.make_async_copy(
+            res_ref.at[pl.ds(pl.multiple_of(me_t * own, own), own)], res, load_sem.at[0]
+        ),
+        pltpu.make_async_copy(wglu_ref, wglu, load_sem.at[1]),
+        pltpu.make_async_copy(wbr_ref, wbr, load_sem.at[2]),
+    ]
+    for load in loads:
+        load.start()
+
+    step = jnp.exp(ls_ref[...])
+    dec, frq = dec_ref[...], frq_ref[...]
+    mag = jnp.exp(dec * step)
+    ar = mag * jnp.cos(frq * step)
+    ai = mag * jnp.sin(frq * step)
+    den = dec * dec + frq * frq
+    less = ar - 1.0
+    hr = (less * dec + ai * frq) / den
+    hi = (ai * dec - less * frq) / den
+    for g in range(groups):
+        at = slice(g * states, (g + 1) * states)
+        coef[0:1, at] = ar[g : g + 1, :]
+        coef[1:2, at] = ai[g : g + 1, :]
+        coef[2:3, at] = hr[g : g + 1, :]
+        coef[3:4, at] = hi[g : g + 1, :]
+
+    u = u_ref[...]
+    spread = (
+        lax.broadcasted_iota(jnp.int32, (group, width), 1) % group
+        == lax.broadcasted_iota(jnp.int32, (group, width), 0)
+    ).astype(BF16)
+    part = 128
+    row = lax.broadcasted_iota(jnp.int32, (tok, part), 0)
+    row8 = lax.broadcasted_iota(jnp.int32, (8, part), 0)
+    for c in range(lanes // part):
+        at = slice(c * part, (c + 1) * part)
+        own_group = (
+            (lax.broadcasted_iota(jnp.int32, (part, width), 0) + c * part) // states
+            == lax.broadcasted_iota(jnp.int32, (part, width), 1) // group
+        )
+
+        def drive(ref):
+            wide = jnp.dot(ref[at, :].astype(BF16), spread, preferred_element_type=F32)
+            wide = jnp.where(own_group, wide, 0.0).astype(BF16)
+            return lax.dot_general(u, wide, NT, preferred_element_type=F32)
+
+        vr, vi = drive(inr_ref), drive(ini_ref)
+        cr, ci = coef[2:3, at], coef[3:4, at]
+        sr, si = cr * vr - ci * vi, cr * vi + ci * vr
+        pr, pi = coef[0:1, at], coef[1:2, at]
+        tr, ti = jnp.ones((8, part), F32), jnp.zeros((8, part), F32)
+        s = 1
+        while s <= tok:
+            if s <= 8:
+                bit = ((row8 + 1) & s) != 0
+                br, bi = jnp.where(bit, pr, 1.0), jnp.where(bit, pi, 0.0)
+                tr, ti = tr * br - ti * bi, tr * bi + ti * br
+            if s >= 8 and s < tok:
+                tr, ti = (
+                    jnp.concatenate([tr, tr * pr - ti * pi], 0),
+                    jnp.concatenate([ti, tr * pi + ti * pr], 0),
+                )
+            if s < tok:
+                if s < 8:
+                    yr = jnp.where(row >= s, pltpu.roll(sr, s, 0), 0.0)
+                    yi = jnp.where(row >= s, pltpu.roll(si, s, 0), 0.0)
+                else:
+                    gap = jnp.zeros((s, part), F32)
+                    yr = jnp.concatenate([gap, sr[: tok - s]], 0)
+                    yi = jnp.concatenate([gap, si[: tok - s]], 0)
+                sr, si = sr + (pr * yr - pi * yi), si + (pr * yi + pi * yr)
+            pr, pi = pr * pr - pi * pi, 2.0 * pr * pi
+            s *= 2
+        xr[:, at], xi[:, at] = sr, si
+        pr_all[:, at], pi_all[:, at] = tr, ti
+        fin[0:1, at] = sr[tok - 1 : tok]
+        fin[1:2, at] = si[tok - 1 : tok]
+
+    greet(n_sp, n_tp, me_s, me_t)
+    ends = []
+    for d in range(1, n_sp):
+        copy = pltpu.make_async_remote_copy(
+            src_ref=fin, dst_ref=fin_in.at[d - 1], send_sem=fs.at[d - 1], recv_sem=fr.at[d - 1],
+            device_id={"sp": lax.rem(me_s + d, n_sp)}, device_id_type=MESH,
+        )
+        copy.start()
+        ends.append(copy)
+
+    spread = (
+        lax.broadcasted_iota(jnp.int32, (states, lanes), 1) % states
+        == lax.broadcasted_iota(jnp.int32, (states, lanes), 0)
+    ).astype(BF16)
+    own_group = (
+        lax.broadcasted_iota(jnp.int32, (width, lanes), 0) // group
+        == lax.broadcasted_iota(jnp.int32, (width, lanes), 1) // states
+    )
+
+    def readout(ref):
+        wide = jnp.dot(ref[...].astype(BF16), spread, preferred_element_type=F32)
+        return jnp.where(own_group, wide, 0.0).astype(BF16)
+
+    outr, outi = readout(outr_ref), readout(outi_ref)
+    for copy in ends:
+        copy.wait()
+    er, ei = pr_all[tok - 1 : tok, :], pi_all[tok - 1 : tok, :]
+    pr, pi = jnp.ones((1, lanes), F32), jnp.zeros((1, lanes), F32)
+    cr, ci = jnp.zeros((1, lanes), F32), jnp.zeros((1, lanes), F32)
+    for d in range(1, n_sp):
+        fr_, fi_ = fin_in[d - 1, 0:1, :], fin_in[d - 1, 1:2, :]
+        reached = me_s >= d
+        cr = cr + jnp.where(reached, pr * fr_ - pi * fi_, 0.0)
+        ci = ci + jnp.where(reached, pr * fi_ + pi * fr_, 0.0)
+        pr, pi = pr * er - pi * ei, pr * ei + pi * er
+    tr, ti = pr_all[...], pi_all[...]
+    sr = (xr[...] + (tr * cr - ti * ci)).astype(BF16)
+    si = (xi[...] + (tr * ci + ti * cr)).astype(BF16)
+    y = lax.dot_general(sr, outr, NT, preferred_element_type=F32) - lax.dot_general(
+        si, outi, NT, preferred_element_type=F32
+    )
+    y = jax.nn.gelu(y + skip_ref[...] * u.astype(F32))
+    mo[...] = y.astype(BF16).reshape(n_tp, own, width)
+    turns = []
+    for d in range(1, n_tp):
+        to = lax.rem(me_t + d, n_tp)
+        copy = pltpu.make_async_remote_copy(
+            src_ref=mo.at[to], dst_ref=rows_in.at[d - 1], send_sem=rs.at[d - 1],
+            recv_sem=rr.at[d - 1], device_id={"tp": to}, device_id_type=MESH,
+        )
+        copy.start()
+        turns.append(copy)
+    for load in loads:
+        load.wait()
+
+    def source(d):
+        return pl.ds(pl.multiple_of(lax.rem(me_t + n_tp - d, n_tp) * width, width), width)
+
+    blocks = [mo[me_t]]
+    pre = bglu_ref[...] + jnp.dot(blocks[0], wglu[source(0), :], preferred_element_type=F32)
+    for d in range(1, n_tp):
+        turns[d - 1].wait()
+        blocks.append(rows_in[d - 1])
+        pre = pre + jnp.dot(blocks[d], wglu[source(d), :], preferred_element_type=F32)
+    glu[...] = pre
+    stream = res[...].astype(F32)
+    for d in range(n_tp):
+        gate = jax.nn.sigmoid(glu[:, source(d)])
+        gated = (blocks[d].astype(F32) * gate).astype(BF16)
+        stream = stream + jnp.dot(gated, wbr[source(d), :], preferred_element_type=F32)
+    stream_ref[...] = stream
+    scale = lax.rsqrt(jnp.mean(stream * stream, axis=-1, keepdims=True) + EPS)
+    normed_ref[...] = (stream * scale * gain_ref[...]).astype(BF16)
+
+
+def pieces(total, count):
+    tiles = total // 128
+    cuts = [128 * (tiles * k // count) for k in range(count)] + [total]
+    return [(a, b) for a, b in zip(cuts[:-1], cuts[1:])]
+
+
+CHUNKS = 3
+
+
+def ffn_kernel(
+    n_sp, n_tp,
+    normed_ref, stream_ref, wg_ref, wu_ref, wd_ref,
+    out_ref,
+    wg, wu, wd, x, part_out, part_in, h, yt_out, yt_in, z_out, z_in,
+    load_sem, as_, ar_, bs, br, cs, cr, ds, dr, es, er, gs, gr,
+):
+    me_s, me_t = lax.axis_index("sp"), lax.axis_index("tp")
+    own, width = normed_ref.shape
+    depth, hid = wg_ref.shape
+    cols = wd_ref.shape[1]
+    cuts = pieces(hid, CHUNKS)
+    loads = [
+        pltpu.make_async_copy(a, b, load_sem.at[k])
+        for k, (a, b) in enumerate(((wg_ref, wg), (wu_ref, wu), (wd_ref, wd)))
+    ]
+    for load in loads:
+        load.start()
+    greet(n_sp, n_tp, me_s, me_t)
+
+    def send(src, dst, ss, rs, **to):
+        copy = pltpu.make_async_remote_copy(
+            src_ref=src, dst_ref=dst, send_sem=ss, recv_sem=rs, device_id=to, device_id_type=MESH
+        )
+        copy.start()
+        return copy
+
+    def col(s, size):
+        return pl.ds(pl.multiple_of(s * size, size), size)
+
+    turns = []
+    for d in range(1, n_sp):
+        to = lax.rem(me_s + d, n_sp)
+        turns.append(
+            send(normed_ref.at[:, col(to, depth)], x.at[d, 0], as_.at[d - 1], ar_.at[d - 1], sp=to)
+        )
+    x[0, 0] = normed_ref[:, col(me_s, depth)]
+    shares = []
+    for k in range(n_sp):
+        if k:
+            turns[k - 1].wait_recv()
+        for d in range(1, n_tp):
+            src = normed_ref.at[:, col(me_s, depth)] if k == 0 else x.at[k, 0]
+            shares.append(
+                send(src, x.at[k, d], bs.at[k, d - 1], br.at[k, d - 1],
+                     tp=lax.rem(me_t + d, n_tp))
+            )
+    loads[0].wait()
+    loads[1].wait()
+    rows = n_tp * own
+    far = list(range(1, n_sp))
+    parts = {}
+    blocks = {}
+    for j, (a, b) in enumerate(cuts):
+        for k in far:
+            if j == 0:
+                for d in range(1, n_tp):
+                    shares[k * (n_tp - 1) + d - 1].wait_recv()
+            block = x[k].reshape(rows, depth)
+            part_out[k - 1, 0, :, a:b] = jnp.dot(
+                block, wg[:, a:b], preferred_element_type=F32
+            ).astype(BF16)
+            part_out[k - 1, 1, :, a:b] = jnp.dot(
+                block, wu[:, a:b], preferred_element_type=F32
+            ).astype(BF16)
+            parts[j, k] = send(
+                part_out.at[k - 1, :, :, pl.ds(a, b - a)], part_in.at[k - 1, :, :, pl.ds(a, b - a)],
+                cs.at[j, k - 1], cr.at[j, k - 1], sp=lax.rem(me_s + n_sp - k, n_sp),
+            )
+    for d in range(1, n_tp):
+        shares[d - 1].wait_recv()
+    mine = x[0].reshape(rows, depth)
+    spreads = {}
+    for j, (a, b) in enumerate(cuts):
+        gate = jnp.dot(mine, wg[:, a:b], preferred_element_type=F32)
+        up = jnp.dot(mine, wu[:, a:b], preferred_element_type=F32)
+        for k in far:
+            parts[j, k].wait_recv()
+            gate = gate + part_in[k - 1, 0, :, a:b].astype(F32)
+            up = up + part_in[k - 1, 1, :, a:b].astype(F32)
+        h[0, :, a:b] = (jax.nn.silu(gate) * up).astype(BF16)
+        for k in far:
+            spreads[j, k] = send(
+                h.at[0, :, pl.ds(a, b - a)], h.at[k, :, pl.ds(a, b - a)],
+                ds.at[j, k - 1], dr.at[j, k - 1], sp=lax.rem(me_s + k, n_sp),
+            )
+    loads[2].wait()
+    sums = []
+    kept = []
+    for k in range(n_sp):
+        if k:
+            for j in range(len(cuts)):
+                spreads[j, k].wait_recv()
+        y = jnp.dot(h[k], wd[...], preferred_element_type=F32).reshape(n_tp, own, cols)
+        kept.append(y[0])
+        for d in range(1, n_tp):
+            yt_out[k, d - 1] = y[d].astype(BF16)
+            sums.append(
+                send(yt_out.at[k, d - 1], yt_in.at[k, d - 1], es.at[k, d - 1], er.at[k, d - 1],
+                     tp=lax.rem(me_t + n_tp - d, n_tp))
+            )
+    back = []
+    for k in far + [0]:
+        z = kept[k]
+        for d in range(1, n_tp):
+            sums[k * (n_tp - 1) + d - 1].wait_recv()
+            z = z + yt_in[k, d - 1].astype(F32)
+        if k:
+            z_out[k - 1] = z.astype(BF16)
+            back.append(
+                send(z_out.at[k - 1], z_in.at[k - 1], gs.at[k - 1], gr.at[k - 1],
+                     sp=lax.rem(me_s + n_sp - k, n_sp))
+            )
+        else:
+            at = col(me_s, cols)
+            out_ref[:, at] = (stream_ref[:, at] + z).astype(BF16)
+    for k in far:
+        back[k - 1].wait_recv()
+        at = col(lax.rem(me_s + k, n_sp), cols)
+        out_ref[:, at] = (stream_ref[:, at] + z_in[k - 1].astype(F32)).astype(BF16)
+    for copy in turns + shares + list(parts.values()) + list(spreads.values()) + sums + back:
+        copy.wait_send()
+
+
+def moved_rows(
+    ssm_input, residual_in, log_step, decay_real, freq, in_real, in_imag, out_real, out_imag,
+    skip, w_glu, b_glu, w_branch, norm_gain, w_gate, w_up, w_down,
+):
+    n_sp, n_tp = lax.axis_size("sp"), lax.axis_size("tp")
+    tok, width = ssm_input.shape
+    groups, states = decay_real.shape
+    group = in_real.shape[2]
+    lanes = groups * states
+    own = tok // n_tp
+    chan, d_model = w_branch.shape
+    depth, hid = w_gate.shape
+    cols = w_down.shape[1]
+    vm = pl.BlockSpec(memory_space=pltpu.VMEM)
+    hbm = pl.BlockSpec(memory_space=pl.ANY)
+    dma = pltpu.SemaphoreType.DMA
+    normed, stream = pl.pallas_call(
+        functools.partial(mixer_kernel, n_sp, n_tp),
+        out_shape=(
+            jax.ShapeDtypeStruct((own, d_model), BF16),
+            jax.ShapeDtypeStruct((own, d_model), F32),
+        ),
+        in_specs=[vm, hbm] + [vm] * 8 + [hbm, vm, hbm, vm],
+        out_specs=(vm, vm),
+        scratch_shapes=[
+            pltpu.VMEM((chan, chan), BF16),
+            pltpu.VMEM((chan, d_model), BF16),
+            pltpu.VMEM((own, d_model), BF16),
+            pltpu.VMEM((8, lanes), F32),
+            pltpu.VMEM((tok, lanes), F32),
+            pltpu.VMEM((tok, lanes), F32),
+            pltpu.VMEM((tok, lanes), F32),
+            pltpu.VMEM((tok, lanes), F32),
+            pltpu.VMEM((2, lanes), F32),
+            pltpu.VMEM((n_sp - 1, 2, lanes), F32),
+            pltpu.VMEM((n_tp, own, width), BF16),
+            pltpu.VMEM((n_tp - 1, own, width), BF16),
+            pltpu.VMEM((own, chan), F32),
+            dma((3,)),
+            dma((n_sp - 1,)),
+            dma((n_sp - 1,)),
+            dma((n_tp - 1,)),
+            dma((n_tp - 1,)),
+        ],
+        compiler_params=pltpu.CompilerParams(collective_id=0, has_side_effects=True),
+        name="mixer",
+    )(
+        ssm_input, residual_in, log_step[:, None], decay_real, freq,
+        in_real.reshape(lanes, group), in_imag.reshape(lanes, group),
+        out_real.reshape(width, states), out_imag.reshape(width, states),
+        skip[None], w_glu, b_glu[None], w_branch, norm_gain[None],
+    )
+    return pl.pallas_call(
+        functools.partial(ffn_kernel, n_sp, n_tp),
+        out_shape=jax.ShapeDtypeStruct((own, d_model), BF16),
+        in_specs=[vm, vm, hbm, hbm, hbm],
+        out_specs=vm,
+        scratch_shapes=[
+            pltpu.VMEM((depth, hid), BF16),
+            pltpu.VMEM((depth, hid), BF16),
+            pltpu.VMEM((hid, cols), BF16),
+            pltpu.VMEM((n_sp, n_tp, own, depth), BF16),
+            pltpu.VMEM((n_sp - 1, 2, tok, hid), BF16),
+            pltpu.VMEM((n_sp - 1, 2, tok, hid), BF16),
+            pltpu.VMEM((n_sp, tok, hid), BF16),
+            pltpu.VMEM((n_sp, n_tp - 1, own, cols), BF16),
+            pltpu.VMEM((n_sp, n_tp - 1, own, cols), BF16),
+            pltpu.VMEM((n_sp - 1, own, cols), BF16),
+            pltpu.VMEM((n_sp - 1, own, cols), BF16),
+            dma((3,)),
+        ]
+        + [dma((n_sp - 1,))] * 2
+        + [dma((n_sp, n_tp - 1))] * 2
+        + [dma((CHUNKS, n_sp - 1))] * 4
+        + [dma((n_sp, n_tp - 1))] * 2
+        + [dma((n_sp - 1,))] * 2,
+        compiler_params=pltpu.CompilerParams(collective_id=1, has_side_effects=True),
+        name="feed_forward",
+    )(normed, stream, w_gate, w_up, w_down)
+
+
+def per_device(*arguments):
+    tok = arguments[0].shape[0]
+    few = lax.axis_size("sp") * tok <= 1024
+    return (moved_rows if few else gathered_weights)(*arguments)
+
+
 def solution(mesh):
     placed = (
         P(("grp", "sp"), "tp"),

time: 370 us -> 140 us (0.38)
  waiting for transfers between devices: 196 us -> 0 us
  Pallas kernels: 0 us -> 134 us
  blocking collectives: 71 us -> 0 us
  local copies, waits for them, and re-layouts: 35 us -> 6.72 us
  matrix products: 24.9 us -> 0 us
  other arithmetic: 24.5 us -> 0 us
  between operations: 13.4 us -> 0.02 us
    all_gather x3 -> x0, waiting for transfers between devices: 170 us -> none  [the longest x1 107 us: per_device(): down_whole = lax.all_gather(w_down, 'sp', axis=1, tiled=True)]
    pallas_call x0 -> x2, Pallas kernels: none -> 134 us  [the longest x1 117 us: moved_rows(): pl.pallas_call(functools.partial(ffn_kernel, n_sp, n_tp), out_shape=jax.S...]
    all_gather x5 -> x0, blocking collectives: 71 us -> none  [the longest x4 64 us: prefix(): everything = jax.tree.map(lambda part: lax.all_gather(part, axis), shard)]
    dot_general x7 -> x0, matrix products: 24.9 us -> none  [the longest x1 7.24 us: per_device(): jnp.dot(hidden, down_whole, preferred_element_type=jnp.float32)]
    dynamic_update_slice x16 -> x0, local copies, waits for them, and re-layouts: 22.3 us -> none  [local_states(): lax.scan(carry_step, (zeros, zeros), (inner_re[:, -1], inner_im[:, -1]))]
    reduce_scatter x1 -> x0, waiting for transfers between devices: 20 us -> none  [per_device(): lax.psum_scatter(jnp.dot(hidden, down_whole, preferred_element_type=jnp.f...]
    add x18 -> x0, other arithmetic: 7.51 us -> none  [the longest x1 5.43 us: per_device(): state_im = local_im + pow_re * carried[3][None] + pow_im * carried[2][None]]
    reduce_sum x1 -> x0, other arithmetic: 6.2 us -> none  [local_states(): jnp.sum(table_re[None] * block_im + table_im[None] * block_re, axis=2)]
  transfers between devices with their start and end apart: 5 -> 0, of which waited for: 4 -> 0; matrix products, arithmetic and copies ran while one was open for 21% -> 0% of each run, Pallas kernels for 0% -> 0%
where the time goes in v1:
time: 140 us
  Pallas kernels  134 us (96%)
  local copies, waits for them, and re-layouts  6.72 us (5%)
    pallas_call x1, Pallas kernels, moved_rows(): pl.pallas_call(functools.partial(ffn_kernel, n_sp, n_tp), out_shape=jax.S...  117 us
    pallas_call x1, Pallas kernels, moved_rows(): pl.pallas_call(functools.partial(mixer_kernel, n_sp, n_tp), out_shape=(ja...  16.5 us
    unnamed x3, local copies, waits for them, and re-layouts  5.39 us

profile of v1, /device:TPU:0, one launch (start us, length us, event | category | flops | bytes accessed | tf_op | source)
XLA Modules:
  0.0 140.3 jit_solution(1859069155285355364)
XLA Ops:
  0.0 1.3 copy.20.ls_ref
  1.3 1.9 %copy.18 = f32[16,64,16]{2,1,0:T(8,128)} copy(f32[16,64,16]{1,2,0:T(8,128)} %param.22) | data formatting | bytes 131072 | tf_op args[5]
  3.2 1.9 %copy.19 = f32[16,64,16]{2,1,0:T(8,128)} copy(f32[16,64,16]{1,2,0:T(8,128)} %param.23) | data formatting | bytes 131072 | tf_op args[6]
  5.2 16.5 %mixer.1 = (bf16[32,2048]{1,0:T(8,128)(2,1)}, f32[32,2048]{1,0:T(8,128)}) custom-call(bf16[128,256]{1,0:T(8,128)(2,1)} %u_ref.1, bf16[128,2048]{1,0:T(8,128)(2,1)} %res_ref.1, f32[16,1]{1,0:T(8,128)} %copy.20.ls_ref, f32[16,64]{1,0:T(8,128)} %dec_ref.1, f32[16,64]{1,0:T(8,128)} %frq_ref.1, f32[1024,16]{1,0:T(8,128)} %bitcast.8, f32[1024,16]{1,0:T(8,128)} %bitcast.9, ...), custom_call_target="tpu_custom_call" | custom-call | tf_op jit(solution)/shard_map/mixer/pallas_call | solution.py:535
  21.6 117.1 %feed_forward.1 = bf16[32,2048]{1,0:T(8,128)(2,1)} custom-call(bf16[32,2048]{1,0:T(8,128)(2,1)} %get-tuple-element.7.normed_ref, f32[32,2048]{1,0:T(8,128)} %get-tuple-element.8.stream_ref, bf16[512,1408]{1,0:T(8,128)(2,1)} %wg_ref.1, bf16[512,1408]{1,0:T(8,128)(2,1)} %wu_ref.1, bf16[1408,512]{1,0:T(8,128)(2,1)} %wd_ref.1), custom_call_target="tpu_custom_call" | custom-call | tf_op jit(solution)/shard_map/feed_forward/pallas_call | solution.py:571
  138.7 1.6 %copy.22 = bf16[32,2048]{1,0:T(8,128)(2,1)} copy(bf16[32,2048]{1,0:T(8,128)(2,1)} %feed_forward.1) | data formatting | bytes 262144

commit v2 on v0

--- a/solution.py
+++ b/solution.py
@@ -1,8 +1,11 @@
+import functools
 import math
 
 import jax
 import jax.numpy as jnp
 from jax import lax
+from jax.experimental import pallas as pl
+from jax.experimental.pallas import tpu as pltpu
 from jax.sharding import PartitionSpec as P
 
 EPS = 1e-06
@@ -121,7 +124,7 @@
     return (stream * scale_rows * norm_gain).astype(jnp.bfloat16)
 
 
-def per_device(
+def gathered_weights(
     ssm_input,
     residual_in,
     log_step,
@@ -194,6 +197,546 @@
     return (stream + summed).astype(jnp.bfloat16)
 
 
+MESH = pl.DeviceIdType.MESH
+F32 = jnp.float32
+BF16 = jnp.bfloat16
+NT = (((1,), (1,)), ((), ()))
+
+
+def greet(sizes, place):
+    barrier = pltpu.get_barrier_semaphore()
+    for axis in sizes:
+        for d in range(1, sizes[axis]):
+            pl.semaphore_signal(
+                barrier, inc=1, device_id={axis: lax.rem(place[axis] + d, sizes[axis])},
+                device_id_type=MESH,
+            )
+    pl.semaphore_wait(barrier, sum(sizes.values()) - len(sizes))
+
+
+def send(src, dst, ss, rs, **to):
+    copy = pltpu.make_async_remote_copy(
+        src_ref=src, dst_ref=dst, send_sem=ss, recv_sem=rs, device_id=to, device_id_type=MESH
+    )
+    copy.start()
+    return copy
+
+
+def aligned(index, size):
+    return pl.ds(pl.multiple_of(index * size, size), size)
+
+
+def mixer(
+    n_sp, n_tp, during,
+    u_ref, res_ref, ls_ref, dec_ref, frq_ref, inr_ref, ini_ref, outr_ref, outi_ref,
+    skip_ref, wglu_ref, bglu_ref, wbr_ref, gain_ref,
+    normed_ref, stream_ref,
+    wglu, wbr, res, coef, xr, xi, pr_all, pi_all, fin, fin_in, mo, rows_in, glu,
+    load_sem, fs, fr, rs, rr,
+):
+    me_s, me_t = lax.axis_index("sp"), lax.axis_index("tp")
+    tok, width = u_ref.shape
+    groups, states = dec_ref.shape
+    group = width // groups
+    lanes = groups * states
+    own = tok // n_tp
+    loads = [
+        pltpu.make_async_copy(
+            res_ref.at[pl.ds(pl.multiple_of(me_t * own, own), own)], res, load_sem.at[0]
+        ),
+        pltpu.make_async_copy(wglu_ref, wglu, load_sem.at[1]),
+        pltpu.make_async_copy(wbr_ref, wbr, load_sem.at[2]),
+    ]
+    for load in loads:
+        load.start()
+
+    same = lax.broadcasted_iota(jnp.int32, (groups, groups), 0) == lax.broadcasted_iota(
+        jnp.int32, (groups, groups), 1
+    )
+    step = jnp.exp(jnp.sum(jnp.where(same, ls_ref[...], 0.0), axis=1, keepdims=True))
+    dec, frq = dec_ref[...], frq_ref[...]
+    mag = jnp.exp(dec * step)
+    ar = mag * jnp.cos(frq * step)
+    ai = mag * jnp.sin(frq * step)
+    den = dec * dec + frq * frq
+    less = ar - 1.0
+    hr = (less * dec + ai * frq) / den
+    hi = (ai * dec - less * frq) / den
+    for g in range(groups):
+        at = slice(g * states, (g + 1) * states)
+        coef[0:1, at] = ar[g : g + 1, :]
+        coef[1:2, at] = ai[g : g + 1, :]
+        coef[2:3, at] = hr[g : g + 1, :]
+        coef[3:4, at] = hi[g : g + 1, :]
+
+    u = u_ref[...]
+    part = 128
+    spread = (
+        lax.broadcasted_iota(jnp.int32, (states, part), 1) % states
+        == lax.broadcasted_iota(jnp.int32, (states, part), 0)
+    ).astype(BF16)
+    rows_group = lax.broadcasted_iota(jnp.int32, (width, part), 0) // group
+    lane_group = lax.broadcasted_iota(jnp.int32, (width, part), 1) // states
+
+    def spread_out(ref):
+        return jnp.dot(ref[...].astype(BF16), spread, preferred_element_type=F32)
+
+    def only(wide, c):
+        return jnp.where(rows_group == lane_group + c * (part // states), wide, 0.0).astype(BF16)
+
+    in_r, in_i = spread_out(inr_ref), spread_out(ini_ref)
+    row = lax.broadcasted_iota(jnp.int32, (tok, part), 0)
+    row8 = lax.broadcasted_iota(jnp.int32, (8, part), 0)
+    for c in range(lanes // part):
+        at = slice(c * part, (c + 1) * part)
+        vr = jnp.dot(u, only(in_r, c), preferred_element_type=F32)
+        vi = jnp.dot(u, only(in_i, c), preferred_element_type=F32)
+        cr, ci = coef[2:3, at], coef[3:4, at]
+        sr, si = cr * vr - ci * vi, cr * vi + ci * vr
+        pr, pi = coef[0:1, at], coef[1:2, at]
+        tr, ti = jnp.ones((8, part), F32), jnp.zeros((8, part), F32)
+        s = 1
+        while s <= tok:
+            if s <= 8:
+                bit = ((row8 + 1) & s) != 0
+                br, bi = jnp.where(bit, pr, 1.0), jnp.where(bit, pi, 0.0)
+                tr, ti = tr * br - ti * bi, tr * bi + ti * br
+            if s >= 8 and s < tok:
+                tr, ti = (
+                    jnp.concatenate([tr, tr * pr - ti * pi], 0),
+                    jnp.concatenate([ti, tr * pi + ti * pr], 0),
+                )
+            if s < tok:
+                if s < 8:
+                    yr = jnp.where(row >= s, pltpu.roll(sr, s, 0), 0.0)
+                    yi = jnp.where(row >= s, pltpu.roll(si, s, 0), 0.0)
+                else:
+                    gap = jnp.zeros((s, part), F32)
+                    yr = jnp.concatenate([gap, sr[: tok - s]], 0)
+                    yi = jnp.concatenate([gap, si[: tok - s]], 0)
+                sr, si = sr + (pr * yr - pi * yi), si + (pr * yi + pi * yr)
+            pr, pi = pr * pr - pi * pi, 2.0 * pr * pi
+            s *= 2
+        xr[:, at], xi[:, at] = sr, si
+        pr_all[:, at], pi_all[:, at] = tr, ti
+        fin[0:1, at] = sr[tok - 1 : tok]
+        fin[1:2, at] = si[tok - 1 : tok]
+
+    ends = []
+    for d in range(1, n_sp):
+        copy = pltpu.make_async_remote_copy(
+            src_ref=fin, dst_ref=fin_in.at[d - 1], send_sem=fs.at[d - 1], recv_sem=fr.at[d - 1],
+            device_id={"sp": lax.rem(me_s + d, n_sp)}, device_id_type=MESH,
+        )
+        copy.start()
+        ends.append(copy)
+
+    out_r, out_i = spread_out(outr_ref), spread_out(outi_ref)
+    outr = jnp.concatenate([only(out_r, c) for c in range(lanes // part)], axis=1)
+    outi = jnp.concatenate([only(out_i, c) for c in range(lanes // part)], axis=1)
+    for copy in ends:
+        copy.wait()
+    er, ei = pr_all[tok - 1 : tok, :], pi_all[tok - 1 : tok, :]
+    pr, pi = jnp.ones((1, lanes), F32), jnp.zeros((1, lanes), F32)
+    cr, ci = jnp.zeros((1, lanes), F32), jnp.zeros((1, lanes), F32)
+    for d in range(1, n_sp):
+        fr_, fi_ = fin_in[d - 1, 0:1, :], fin_in[d - 1, 1:2, :]
+        reached = me_s >= d
+        cr = cr + jnp.where(reached, pr * fr_ - pi * fi_, 0.0)
+        ci = ci + jnp.where(reached, pr * fi_ + pi * fr_, 0.0)
+        pr, pi = pr * er - pi * ei, pr * ei + pi * er
+    tr, ti = pr_all[...], pi_all[...]
+    sr = (xr[...] + (tr * cr - ti * ci)).astype(BF16)
+    si = (xi[...] + (tr * ci + ti * cr)).astype(BF16)
+    y = lax.dot_general(sr, outr, NT, preferred_element_type=F32) - lax.dot_general(
+        si, outi, NT, preferred_element_type=F32
+    )
+    y = jax.nn.gelu(y + skip_ref[...] * u.astype(F32))
+    mo[...] = y.astype(BF16).reshape(n_tp, own, width)
+    turns = []
+    for d in range(1, n_tp):
+        to = lax.rem(me_t + d, n_tp)
+        copy = pltpu.make_async_remote_copy(
+            src_ref=mo.at[to], dst_ref=rows_in.at[d - 1], send_sem=rs.at[d - 1],
+            recv_sem=rr.at[d - 1], device_id={"tp": to}, device_id_type=MESH,
+        )
+        copy.start()
+        turns.append(copy)
+    during()
+    for load in loads:
+        load.wait()
+
+    def source(d):
+        return pl.ds(pl.multiple_of(lax.rem(me_t + n_tp - d, n_tp) * width, width), width)
+
+    blocks = [mo[me_t]]
+    pre = bglu_ref[...] + jnp.dot(blocks[0], wglu[source(0), :], preferred_element_type=F32)
+    for d in range(1, n_tp):
+        turns[d - 1].wait()
+        blocks.append(rows_in[d - 1])
+        pre = pre + jnp.dot(blocks[d], wglu[source(d), :], preferred_element_type=F32)
+    glu[...] = pre
+    stream = res[...].astype(F32)
+    for d in range(n_tp):
+        gate = jax.nn.sigmoid(glu[:, source(d)])
+        gated = (blocks[d].astype(F32) * gate).astype(BF16)
+        stream = stream + jnp.dot(gated, wbr[source(d), :], preferred_element_type=F32)
+    stream_ref[...] = stream
+    scale = lax.rsqrt(jnp.mean(stream * stream, axis=-1, keepdims=True) + EPS)
+    normed_ref[...] = (stream * scale * gain_ref[...]).astype(BF16)
+
+
+def pieces(total, count):
+    tiles = total // 128
+    cuts = [total - 128 * (tiles * k // count) for k in range(count, -1, -1)]
+    cuts[0] = 0
+    return [(a, b) for a, b in zip(cuts[:-1], cuts[1:])]
+
+
+CHUNKS = 4
+DOWN = 2
+
+
+def layer_kernel(sizes, *refs):
+    n_sp, n_tp = sizes["sp"], sizes["tp"]
+    place = {axis: lax.axis_index(axis) for axis in sizes}
+    me_g, me_s, me_t = place["grp"], place["sp"], place["tp"]
+    wg_ref, wu_ref, wd_ref, out_ref = refs[14:18]
+    normed, stream, wgu, wd, x, part_out, part_in, h, y_out, y_in, z_out, z_in = refs[18:30]
+    (load_sem, hs, hr, fs, fr, ks, kr, ls, lr, as_, ar_, bs, br, cs, cr, ds, dr, es, er, gs, gr) = (
+        refs[30:51]
+    )
+    mixer_scratch = refs[51:]
+    own, d_model = normed.shape
+    depth, hid = wg_ref.shape
+    cols = wd_ref.shape[1]
+    half = me_s // 2
+    inner = me_s % 2 != half
+    hub = half + 1
+    far_hub = 2 - half
+    edge = 3 * half
+    cuts = pieces(hid, CHUNKS)
+    span = depth // 2
+    rows_down = hid // 2 // DOWN
+    edge_row = (edge % 2) * depth
+    edge_col = pl.ds(pl.multiple_of((edge % 2) * cols, cols), cols)
+
+    def edge_rows(g):
+        return pl.ds(pl.multiple_of(edge_row + g * span, span), span)
+
+    def down_rows(g, k):
+        return pl.ds(pl.multiple_of((g * DOWN + k) * rows_down, rows_down), rows_down)
+
+    def handed(j, start=True):
+        a, b = cuts[j]
+        copies = []
+        for k, ref in enumerate((wg_ref, wu_ref)):
+            copies.append(
+                pltpu.make_async_remote_copy(
+                    src_ref=ref.at[aligned(me_g, span), pl.ds(a, b - a)],
+                    dst_ref=wgu.at[k, edge_rows(me_g), pl.ds(a, b - a)],
+                    send_sem=hs.at[j, k], recv_sem=hr.at[j, k],
+                    device_id={"sp": hub}, device_id_type=MESH,
+                )
+            )
+        return copies
+
+    def handed_down(k):
+        return pltpu.make_async_remote_copy(
+            src_ref=wd_ref.at[down_rows(me_g, k), :],
+            dst_ref=wd.at[down_rows(me_g, k), edge_col],
+            send_sem=ks.at[k], recv_sem=kr.at[k], device_id={"sp": hub}, device_id_type=MESH,
+        )
+
+    def shared(j):
+        a, b = cuts[j]
+        piece = wgu.at[:, edge_rows(me_g), pl.ds(a, b - a)]
+        return pltpu.make_async_remote_copy(
+            src_ref=piece, dst_ref=piece, send_sem=fs.at[j], recv_sem=fr.at[j],
+            device_id={"grp": 1 - me_g}, device_id_type=MESH,
+        )
+
+    def shared_down(k):
+        piece = wd.at[down_rows(me_g, k), edge_col]
+        return pltpu.make_async_remote_copy(
+            src_ref=piece, dst_ref=piece, send_sem=ls.at[k], recv_sem=lr.at[k],
+            device_id={"grp": 1 - me_g}, device_id_type=MESH,
+        )
+
+    def hand(j):
+        for copy in handed(j):
+            copy.start()
+
+    def share(j):
+        for copy in handed(j):
+            copy.wait_recv()
+        shared(j).start()
+
+    own_loads = [
+        pltpu.make_async_copy(
+            ref, wgu.at[k, aligned(me_s % 2, depth), :], load_sem.at[k]
+        )
+        for k, ref in enumerate((wg_ref, wu_ref))
+    ] + [pltpu.make_async_copy(wd_ref, wd.at[:, aligned(me_s % 2, cols)], load_sem.at[2])]
+
+    greet(sizes, place)
+
+    @pl.when(jnp.logical_not(inner))
+    def _():
+        hand(0)
+        hand(1)
+
+    @pl.when(inner)
+    def _():
+        for load in own_loads:
+            load.start()
+
+    def during():
+        @pl.when(jnp.logical_not(inner))
+        def _():
+            hand(2)
+
+        @pl.when(inner)
+        def _():
+            share(0)
+
+    mixer(n_sp, n_tp, during, *refs[:14], normed, stream, *mixer_scratch)
+
+    pair = 2 * depth
+
+    def to_hub(q):
+        return pltpu.make_async_remote_copy(
+            src_ref=normed.at[:, pl.ds(q * pair, pair)], dst_ref=x.at[me_s, 0],
+            send_sem=as_.at[q], recv_sem=ar_.at[me_s],
+            device_id={"sp": q + 1}, device_id_type=MESH,
+        )
+
+    for q in range(2):
+        @pl.when(me_s != q + 1)
+        def _():
+            to_hub(q).start()
+
+    mate = me_t + 1 - 2 * (me_t % 2)
+    across = lax.rem(me_t + 2, n_tp)
+
+    def from_hub(s, r, ref, sem):
+        return pltpu.make_async_remote_copy(
+            src_ref=ref, dst_ref=z_in.at[r], send_sem=gs.at[s], recv_sem=gr.at[r],
+            device_id={"sp": s}, device_id_type=MESH,
+        )
+
+    @pl.when(jnp.logical_not(inner))
+    def _():
+        hand(3)
+        for j in range(CHUNKS):
+            for copy in handed(j):
+                copy.wait_send()
+        for k in range(DOWN):
+            handed_down(k).start()
+
+    @pl.when(inner)
+    def _():
+        x[me_s, 0] = normed[:, aligned(half, pair)]
+        shares = {}
+        order = [hub, edge, far_hub, 3 - edge]
+
+        def arrival(s):
+            return pltpu.make_async_remote_copy(
+                src_ref=x.at[s, 0], dst_ref=x.at[s, 0], send_sem=as_.at[0], recv_sem=ar_.at[s],
+                device_id={"sp": far_hub}, device_id_type=MESH,
+            )
+
+        def block(s, src, r, slot, to):
+            return send(src, x.at[s, slot], bs.at[s, r], br.at[s, r], tp=to)
+
+        for i, s in enumerate(order):
+            if i:
+                arrival(s).wait_recv()
+            src = normed.at[:, aligned(half, pair)] if i == 0 else x.at[s, 0]
+            shares[i, 1] = block(s, src, 0, 2, across)
+            shares[i, 0] = block(s, src, 1, 1, mate)
+        share(1)
+        for i, s in enumerate(order):
+            shares[i, 1].wait_recv()
+            shares[i, 2] = block(s, x.at[s, 2], 2, 3, mate)
+        own_loads[0].wait()
+        own_loads[1].wait()
+        rows = 2 * n_tp * own
+        for i, s in enumerate(order):
+            shares[i, 0].wait_recv()
+            shares[i, 2].wait_recv()
+        theirs = x[aligned(1 - half, 2)].reshape(rows, pair)
+        parts = []
+        for j, (a, b) in enumerate(cuts):
+            if j >= 1 and j + 1 < CHUNKS:
+                share(j + 1)
+            shared(j).wait_recv()
+            for k in range(2):
+                part_out[k, :, a:b] = jnp.dot(
+                    theirs, wgu[k, :, a:b], preferred_element_type=F32
+                ).astype(BF16)
+            parts.append(
+                send(part_out.at[:, :, pl.ds(a, b - a)], part_in.at[:, :, pl.ds(a, b - a)],
+                     cs.at[j], cr.at[j], sp=far_hub)
+            )
+        mine = x[aligned(half, 2)].reshape(rows, pair)
+        spreads = []
+        for j, (a, b) in enumerate(cuts):
+            gate = jnp.dot(mine, wgu[0, :, a:b], preferred_element_type=F32)
+            up = jnp.dot(mine, wgu[1, :, a:b], preferred_element_type=F32)
+            parts[j].wait_recv()
+            gate = gate + part_in[0, :, a:b].astype(F32)
+            up = up + part_in[1, :, a:b].astype(F32)
+            h[0, :, a:b] = (jax.nn.silu(gate) * up).astype(BF16)
+            spreads.append(
+                send(h.at[0, :, pl.ds(a, b - a)], h.at[1, :, pl.ds(a, b - a)],
+                     ds.at[j], dr.at[j], sp=far_hub)
+            )
+            if j < DOWN:
+                handed_down(j).wait_recv()
+                shared_down(j).start()
+        own_loads[2].wait()
+        for k in range(DOWN):
+            shared_down(k).wait_recv()
+        slots = [0, 1, 2, 3]
+        targets = [me_t, mate, across, 3 - me_t]
+        sums = []
+        kept = []
+        for i in range(2):
+            if i:
+                for spread in spreads:
+                    spread.wait_recv()
+            y = jnp.dot(h[i], wd[...], preferred_element_type=F32).reshape(2, n_tp, own, pair)
+            kept.append(y[:, 0])
+            for r in (2, 3, 1):
+                y_out[i, r - 1] = y[:, r].astype(BF16)
+                sums.append(
+                    send(y_out.at[i, r - 1], y_in.at[i, r - 1], es.at[i, r - 1], er.at[i, r - 1],
+                         tp=targets[r])
+                )
+        backs = []
+        for i in (0, 1):
+            z = kept[i]
+            for n in range(3):
+                sums[3 * i + n].wait_recv()
+            for r in range(1, n_tp):
+                z = z + y_in[i, r - 1].astype(F32)
+            z_out[i] = z.astype(BF16)
+            if i == 0:
+                at = aligned(half, pair)
+                spare = me_s % 2
+                out_ref[:, at] = (stream[:, at] + z_out[0, spare].astype(F32)).astype(BF16)
+                copy = from_hub(edge, half, z_out.at[0, 1 - spare], None)
+                copy.start()
+                backs.append(copy)
+            else:
+                for e in range(2):
+                    copy = from_hub(2 * (1 - half) + e, half, z_out.at[1, e], None)
+                    copy.start()
+                    backs.append(copy)
+        for copy in list(shares.values()) + parts + spreads + sums + backs:
+            copy.wait_send()
+        for j in range(CHUNKS):
+            shared(j).wait_send()
+        for k in range(DOWN):
+            shared_down(k).wait_send()
+
+    for q in range(2):
+        @pl.when(me_s != q + 1)
+        def _():
+            pltpu.make_async_remote_copy(
+                src_ref=z_in.at[q], dst_ref=z_in.at[q], send_sem=gs.at[0], recv_sem=gr.at[q],
+                device_id={"sp": q + 1}, device_id_type=MESH,
+            ).wait_recv()
+            at = pl.ds(q * pair, pair)
+            out_ref[:, at] = (stream[:, at] + z_in[q].astype(F32)).astype(BF16)
+            to_hub(q).wait_send()
+
+    @pl.when(jnp.logical_not(inner))
+    def _():
+        for k in range(DOWN):
+            handed_down(k).wait_send()
+
+
+def moved_rows(
+    ssm_input, residual_in, log_step, decay_real, freq, in_real, in_imag, out_real, out_imag,
+    skip, w_glu, b_glu, w_branch, norm_gain, w_gate, w_up, w_down,
+):
+    sizes = {axis: lax.axis_size(axis) for axis in ("grp", "sp", "tp")}
+    n_sp, n_tp = sizes["sp"], sizes["tp"]
+    tok, width = ssm_input.shape
+    groups, states = decay_real.shape
+    group = in_real.shape[2]
+    lanes = groups * states
+    own = tok // n_tp
+    chan, d_model = w_branch.shape
+    depth, hid = w_gate.shape
+    cols = w_down.shape[1]
+    pair = 2 * depth
+    vm = pl.BlockSpec(memory_space=pltpu.VMEM)
+    hbm = pl.BlockSpec(memory_space=pl.ANY)
+    dma = pltpu.SemaphoreType.DMA
+    vmem = pltpu.VMEM
+    return pl.pallas_call(
+        functools.partial(layer_kernel, sizes),
+        out_shape=jax.ShapeDtypeStruct((own, d_model), BF16),
+        in_specs=[vm, hbm] + [vm] * 8 + [hbm, vm, hbm, vm] + [hbm] * 3,
+        out_specs=vm,
+        scratch_shapes=[
+            vmem((own, d_model), BF16),
+            vmem((own, d_model), F32),
+            vmem((2, pair, hid), BF16),
+            vmem((hid, 2 * cols), BF16),
+            vmem((n_sp, n_tp, own, pair), BF16),
+            vmem((2, 2 * tok, hid), BF16),
+            vmem((2, 2 * tok, hid), BF16),
+            vmem((2, 2 * tok, hid), BF16),
+            vmem((2, n_tp - 1, 2, own, pair), BF16),
+            vmem((2, n_tp - 1, 2, own, pair), BF16),
+            vmem((2, 2, own, pair), BF16),
+            vmem((2, own, pair), BF16),
+            dma((3,)),
+            dma((CHUNKS, 2)), dma((CHUNKS, 2)),
+            dma((CHUNKS,)), dma((CHUNKS,)),
+            dma((DOWN,)), dma((DOWN,)), dma((DOWN,)), dma((DOWN,)),
+            dma((2,)), dma((n_sp,)),
+            dma((n_sp, 3)), dma((n_sp, 3)),
+            dma((CHUNKS,)), dma((CHUNKS,)), dma((CHUNKS,)), dma((CHUNKS,)),
+            dma((2, n_tp - 1)), dma((2, n_tp - 1)),
+            dma((n_sp,)), dma((2,)),
+            vmem((chan, chan), BF16),
+            vmem((chan, d_model), BF16),
+            vmem((own, d_model), BF16),
+            vmem((8, lanes), F32),
+            vmem((tok, lanes), F32),
+            vmem((tok, lanes), F32),
+            vmem((tok, lanes), F32),
+            vmem((tok, lanes), F32),
+            vmem((2, lanes), F32),
+            vmem((n_sp - 1, 2, lanes), F32),
+            vmem((n_tp, own, width), BF16),
+            vmem((n_tp - 1, own, width), BF16),
+            vmem((own, chan), F32),
+            dma((3,)),
+            dma((n_sp - 1,)), dma((n_sp - 1,)),
+            dma((n_tp - 1,)), dma((n_tp - 1,)),
+        ],
+        compiler_params=pltpu.CompilerParams(collective_id=0, has_side_effects=True),
+        name="layer",
+    )(
+        ssm_input, residual_in, log_step[None], decay_real, freq,
+        in_real.swapaxes(1, 2).reshape(width, states),
+        in_imag.swapaxes(1, 2).reshape(width, states),
+        out_real.reshape(width, states), out_imag.reshape(width, states),
+        skip[None], w_glu, b_glu[None], w_branch, norm_gain[None], w_gate, w_up, w_down,
+    )
+
+
+def per_device(*arguments):
+    sizes = tuple(lax.axis_size(axis) for axis in ("grp", "sp", "tp"))
+    return (moved_rows if sizes == (2, 4, 4) else gathered_weights)(*arguments)
+
+
 def solution(mesh):
     placed = (
         P(("grp", "sp"), "tp"),

time: 370 us -> 109 us (0.29)
  waiting for transfers between devices: 196 us -> 0 us
  Pallas kernels: 0 us -> 108 us
  blocking collectives: 71 us -> 0 us
  local copies, waits for them, and re-layouts: 35 us -> 1.57 us
  matrix products: 24.9 us -> 0 us
  other arithmetic: 24.5 us -> 0 us
  between operations: 13.4 us -> 0.01 us
    all_gather x3 -> x0, waiting for transfers between devices: 170 us -> none  [the longest x1 107 us: per_device(): down_whole = lax.all_gather(w_down, 'sp', axis=1, tiled=True)]
    pallas_call x0 -> x1, Pallas kernels: none -> 108 us  [moved_rows(): pl.pallas_call(functools.partial(layer_kernel, sizes), out_shape=jax.Shap...]
    all_gather x5 -> x0, blocking collectives: 71 us -> none  [the longest x4 64 us: prefix(): everything = jax.tree.map(lambda part: lax.all_gather(part, axis), shard)]
    dot_general x7 -> x0, matrix products: 24.9 us -> none  [the longest x1 7.24 us: per_device(): jnp.dot(hidden, down_whole, preferred_element_type=jnp.float32)]
    dynamic_update_slice x16 -> x0, local copies, waits for them, and re-layouts: 22.3 us -> none  [local_states(): lax.scan(carry_step, (zeros, zeros), (inner_re[:, -1], inner_im[:, -1]))]
    reduce_scatter x1 -> x0, waiting for transfers between devices: 20 us -> none  [per_device(): lax.psum_scatter(jnp.dot(hidden, down_whole, preferred_element_type=jnp.f...]
    add x18 -> x0, other arithmetic: 7.51 us -> none  [the longest x1 5.43 us: per_device(): state_im = local_im + pow_re * carried[3][None] + pow_im * carried[2][None]]
    reduce_sum x1 -> x0, other arithmetic: 6.2 us -> none  [local_states(): jnp.sum(table_re[None] * block_im + table_im[None] * block_re, axis=2)]
  transfers between devices with their start and end apart: 5 -> 0, of which waited for: 4 -> 0; matrix products, arithmetic and copies ran while one was open for 21% -> 0% of each run, Pallas kernels for 0% -> 0%
where the time goes in v2:
time: 109 us
  Pallas kernels  108 us (99%)
  local copies, waits for them, and re-layouts  1.57 us (1%)
    pallas_call x1, Pallas kernels, moved_rows(): pl.pallas_call(functools.partial(layer_kernel, sizes), out_shape=jax.Shap...  108 us

profile of v2, /device:TPU:0, one launch (start us, length us, event | category | flops | bytes accessed | tf_op | source)
XLA Modules:
  0.0 109.2 jit_solution(16812543263488741848)
XLA Ops:
  0.0 107.6 %layer.1 = bf16[32,2048]{1,0:T(8,128)(2,1)} custom-call(bf16[128,256]{1,0:T(8,128)(2,1)} %refs_0_.1, bf16[128,2048]{1,0:T(8,128)(2,1)} %refs_1_.1, f32[1,16]{1,0:T(1,128)} %bitcast.19, f32[16,64]{1,0:T(8,128)} %refs_3_.1, f32[16,64]{1,0:T(8,128)} %refs_4_.1, f32[256,64]{1,0:T(8,128)} %bitcast.12, f32[256,64]{1,0:T(8,128)} %bitcast.13, f32[256,64]{1,0:T(8,128)} %bitcast.14, ...), custom_call_target="tpu_custom_call" | custom-call | tf_op jit(solution)/shard_map/layer/pallas_call | solution.py:680
  107.6 1.6 %copy.19 = bf16[32,2048]{1,0:T(8,128)(2,1)} copy(bf16[32,2048]{1,0:T(8,128)(2,1)} %layer.1) | data formatting | bytes 262144

commit v3 on v2

--- a/solution.py
+++ b/solution.py
@@ -536,6 +536,7 @@
 
     @pl.when(inner)
     def _():
+        share(1)
         x[me_s, 0] = normed[:, aligned(half, pair)]
         shares = {}
         order = [hub, edge, far_hub, 3 - edge]
@@ -555,10 +556,10 @@
             src = normed.at[:, aligned(half, pair)] if i == 0 else x.at[s, 0]
             shares[i, 1] = block(s, src, 0, 2, across)
             shares[i, 0] = block(s, src, 1, 1, mate)
-        share(1)
         for i, s in enumerate(order):
             shares[i, 1].wait_recv()
             shares[i, 2] = block(s, x.at[s, 2], 2, 3, mate)
+        share(2)
         own_loads[0].wait()
         own_loads[1].wait()
         rows = 2 * n_tp * own
@@ -568,8 +569,8 @@
         theirs = x[aligned(1 - half, 2)].reshape(rows, pair)
         parts = []
         for j, (a, b) in enumerate(cuts):
-            if j >= 1 and j + 1 < CHUNKS:
-                share(j + 1)
+            if j == 1:
+                share(3)
             shared(j).wait_recv()
             for k in range(2):
                 part_out[k, :, a:b] = jnp.dot(
@@ -592,9 +593,9 @@
                 send(h.at[0, :, pl.ds(a, b - a)], h.at[1, :, pl.ds(a, b - a)],
                      ds.at[j], dr.at[j], sp=far_hub)
             )
-            if j < DOWN:
-                handed_down(j).wait_recv()
-                shared_down(j).start()
+            if 1 <= j <= DOWN:
+                handed_down(j - 1).wait_recv()
+                shared_down(j - 1).start()
         own_loads[2].wait()
         for k in range(DOWN):
             shared_down(k).wait_recv()

time: 109 us -> 109 us (level)
  no operation moved by 1% of the time
where the time goes in v3:
time: 109 us
  Pallas kernels  108 us (99%)
  local copies, waits for them, and re-layouts  1.57 us (1%)
    pallas_call x1, Pallas kernels, moved_rows(): pl.pallas_call(functools.partial(layer_kernel, sizes), out_shape=jax.Shap...  108 us

profile of v3, /device:TPU:0, one launch (start us, length us, event | category | flops | bytes accessed | tf_op | source)
XLA Modules:
  0.0 109.2 jit_solution(6814898843279904640)
XLA Ops:
  0.0 107.6 %layer.1 = bf16[32,2048]{1,0:T(8,128)(2,1)} custom-call(bf16[128,256]{1,0:T(8,128)(2,1)} %refs_0_.1, bf16[128,2048]{1,0:T(8,128)(2,1)} %refs_1_.1, f32[1,16]{1,0:T(1,128)} %bitcast.19, f32[16,64]{1,0:T(8,128)} %refs_3_.1, f32[16,64]{1,0:T(8,128)} %refs_4_.1, f32[256,64]{1,0:T(8,128)} %bitcast.12, f32[256,64]{1,0:T(8,128)} %bitcast.13, f32[256,64]{1,0:T(8,128)} %bitcast.14, ...), custom_call_target="tpu_custom_call" | custom-call | tf_op jit(solution)/shard_map/layer/pallas_call | solution.py:681
  107.6 1.6 %copy.19 = bf16[32,2048]{1,0:T(8,128)(2,1)} copy(bf16[32,2048]{1,0:T(8,128)(2,1)} %layer.1) | data formatting | bytes 262144
